TPU v7x, 512 devices: a whole 4x4x16 slice. The times are simulated.
512 devices in a mesh: fs: 16 (over y, x), tp: 32 (over z, core).
Axes of the slice: x: 4, y: 4, z: 16, core: 2. Of those that a mesh axis runs over, the one named last changes fastest.
Arguments:
- tokens: bfloat16 [8192, 2048], P('fs', 'tp'), may hold values from -6 to 6
- norm_gain: float32 [2048], P('fs'), may hold values from 0.1 to 1.9
- gate_train: float32 [2048, 8192], P('fs', 'tp'), may hold values from -0.125 to 0.125
- up_train: float32 [2048, 8192], P('fs', 'tp'), may hold values from -0.125 to 0.125
- down_train: float32 [8192, 2048], P('fs', 'tp'), may hold values from -0.0625 to 0.0625
Outputs:
- gate_serve: bfloat16 [2048, 8192], P(None, 'tp')
- up_serve: bfloat16 [2048, 8192], P(None, 'tp')
- down_serve: bfloat16 [8192, 2048], P('tp')
- layer_out: bfloat16 [8192, 2048], P(('fs', 'tp'))
All inputs are finite; a program needn't handle non-finite values.
Results may differ from a plain program's by a relative error of at most 0.024.
Values may be sent and summed in bfloat16 or wider, within the bound.
No kernel may reach another device: no remote copies, remote signals or barrier semaphores. Data moves between devices by JAX's collectives and lax.ppermute only.
A program may use at most 64 MiB of HBM per device.

v0:
```python
import jax
import jax.numpy as jnp
from jax import lax
from jax.sharding import Mesh
from jax.sharding import PartitionSpec as P

D = 2048
TP = ("tp_0", "tp_1")
FS_TP = ("fs", "tp_0", "tp_1")
epsilon = 1e-06


def side_by_side(arrays, axis, dim, along):
    both = jnp.concatenate(arrays, axis=along)
    whole, at, finished = (lax.all_gather(both, axis, axis=dim, tiled=True), 0, [])
    for a in arrays:
        finished.append(lax.slice_in_dim(whole, at, at + a.shape[along], axis=along))
        at += a.shape[along]
    return tuple(finished)


def joined_along(pieces, dim):
    shape = list(pieces.shape[1:])
    shape[dim] *= pieces.shape[0]
    return jnp.moveaxis(pieces, 0, dim).reshape(shape)


def copy_for_each(x, axis):
    copies = jnp.broadcast_to(x, (lax.axis_size(axis), *x.shape))
    return lax.all_to_all(copies, axis, split_axis=0, concat_axis=0, tiled=True)


def collect(x, axis, dim):
    return joined_along(copy_for_each(x, axis), dim)


def sum_in_order(pieces, axes, order):
    shape = [lax.axis_size(a) for a in axes]
    pieces = pieces.reshape(*shape, *pieces.shape[1:])
    pieces = pieces.transpose(*order, *range(len(axes), pieces.ndim))
    pieces = pieces.reshape(-1, *pieces.shape[len(axes) :])
    for k in order:
        pieces = lax.psum_scatter(pieces, axes[k], scatter_dimension=0, tiled=True)
    return pieces[0]


def cut_along(x, dim, count):
    before, after = (x.shape[:dim], x.shape[dim + 1 :])
    return jnp.moveaxis(x.reshape(*before, count, -1, *after), dim, 0)


def sum_by_axis(x, axes, order, dim):
    count = lax.axis_size(axes)
    return sum_in_order(cut_along(x, dim, count), axes, order)


def body(tokens, norm_gain, gate_train, up_train, down_train):
    gate_local = (norm_gain[:, None] * gate_train).astype(jnp.bfloat16)
    up_local = (norm_gain[:, None] * up_train).astype(jnp.bfloat16)
    down_local = down_train.astype(jnp.bfloat16)
    features = lax.all_gather(tokens, TP, axis=1, tiled=True)
    wide = features.astype(jnp.float32)
    squares = jnp.sum(wide * wide, axis=1)
    gate_whole, up_whole = side_by_side((gate_local, up_local), "fs", 0, 1)
    gate_sum = jnp.dot(features, gate_whole, preferred_element_type=jnp.float32)
    up_sum = jnp.dot(features, up_whole, preferred_element_type=jnp.float32)
    down_rows = collect(down_local, "fs", 0)
    down_whole = lax.all_to_all(down_rows, TP, split_axis=0, concat_axis=1, tiled=True)
    scale = lax.rsqrt(squares / D + epsilon)[:, None]
    hidden = (jax.nn.silu(gate_sum * scale) * (up_sum * scale)).astype(jnp.bfloat16)
    mixed = (
        sum_by_axis(
            jnp.dot(hidden, down_whole, preferred_element_type=jnp.float32).astype(jnp.bfloat16),
            TP,
            (1, 0),
            0,
        )
        .astype(jnp.float32)
        .astype(jnp.bfloat16)
    )
    return (gate_whole, up_whole, down_whole, mixed)


def solution(mesh):
    finer = Mesh(mesh.devices.reshape(mesh.shape["fs"], 16, 2), ("fs", "tp_0", "tp_1"))
    placed = (P("fs", TP), P("fs"), P("fs", TP), P("fs", TP), P("fs", TP))
    return jax.shard_map(
        body,
        mesh=finer,
        in_specs=placed,
        out_specs=(P(None, TP), P(None, TP), P(TP, None), P(FS_TP, None)),
        check_vma=False,
    )
```

profile of v0, /device:TPU:2, one launch (start us, length us, event | category | flops | bytes accessed | tf_op | source)
XLA Modules:
  0.0 262.0 jit_solution(8087558812155801704)
XLA Ops:
  7.2 0.0 all-gather.3.cloned.1.call-start
  7.2 1.1 multiply_convert_fusion.1
  8.3 0.7 pad_maximum_fusion
  9.0 0.9 convert_element_type.22
  9.9 1.1 broadcast_in_dim.2
  11.0 9.3 %all-to-all-start = ((bf16[16,512,64]{1,2,0:T(8,128)(2,1)}), bf16[16,512,64]{1,2,0:T(8,128)(2,1)S(1)}, u32[]{:S(2)}, u32[]{:S(2)}) async-start(bf16[16,512,64]{1,2,0:T(8,128)(2,1)} %broadcast_in_dim.2), calls=%async_computation | async-start | bytes 2097152 | tf_op jit(solution)/shard_map/all_to_all | solution.py:30
  20.3 0.7 all-gather.5.cloned.1.call-update
  21.0 13.6 %all-to-all-done = bf16[16,512,64]{1,2,0:T(8,128)(2,1)S(1)} async-done(((bf16[16,512,64]{1,2,0:T(8,128)(2,1)}), bf16[16,512,64]{1,2,0:T(8,128)(2,1)S(1)}, u32[]{:S(2)}, u32[]{:S(2)}) %all-to-all-start) | async-done | bytes 1048608 | tf_op jit(solution)/shard_map/all_to_all | solution.py:30
  34.7 0.6 copy.14
  35.2 0.4 all_to_all.18
  35.6 1.6 copy.15
  37.2 15.0 %all-to-all-start.1 = ((bf16[32,256,64]{1,2,0:T(8,128)(2,1)}), bf16[32,256,64]{1,2,0:T(8,128)(2,1)S(1)}, u32[]{:S(2)}, u32[]{:S(2)}) async-start(bf16[32,256,64]{1,2,0:T(8,128)(2,1)} %copy.15), calls=%async_computation.1 | async-start | bytes 2097152 | tf_op jit(solution)/shard_map/all_to_all | solution.py:68
  52.3 0.0 reduce-scatter.3.cloned.1.call-start
  52.3 23.6 %all-gather.3.cloned.1.call-done = bf16[2048,512]{1,0:T(8,128)(2,1)} async-done(((bf16[128,512]{1,0:T(8,128)(2,1)}), bf16[2048,512]{1,0:T(8,128)(2,1)}) %all-gather.3.cloned.1.call-update) | async-done | bytes 2097168 | tf_op jit(solution)/shard_map/all_gather | solution.py:15
  75.9 3.0 %fusion.12 = (bf16[2048,256]{1,0:T(8,128)(2,1)}, bf16[2048,256]{1,0:T(8,128)(2,1)}) fusion(bf16[2048,512]{1,0:T(8,128)(2,1)} %all-gather.3.cloned.1.call-done), kind=kLoop, calls=%fused_computation.20 | loop fusion | bytes 4194304 | tf_op jit(solution)/shard_map/slice | solution.py:17
  78.9 71.5 %all-gather.5.cloned.1.call-done = bf16[512,2048]{0,1:T(8,128)(2,1)} async-done(((bf16[512,64]{0,1:T(8,128)(2,1)}), bf16[512,2048]{0,1:T(8,128)(2,1)}) %all-gather.5.cloned.1.call-update) | async-done | bytes 2097168 | tf_op jit(solution)/shard_map/all_gather | solution.py:61
  150.4 2.2 multiply_reduce_fusion
  152.7 2.8 %fusion.2 = f32[512,256]{0,1:T(8,128)} fusion(bf16[2048,256]{1,0:T(8,128)(2,1)} %get-tuple-element.13, bf16[512,2048]{0,1:T(8,128)(2,1)S(1)} %copy-done, f32[512]{0:T(512)S(1)} %add_rsqrt_fusion), kind=kOutput, calls=%fused_computation.6 | convolution fusion | flops 537001984 | bytes 3672064 | tf_op jit(solution)/shard_map/dot_general | solution.py:65
  155.5 4.2 %convolution_convert_fusion = bf16[512,2048]{1,0:T(8,128)(2,1)} fusion(bf16[256,2048]{0,1:T(8,128)(2,1)S(1)} %bitcast.26, bf16[2048,256]{1,0:T(8,128)(2,1)} %get-tuple-element.12, bf16[512,2048]{0,1:T(8,128)(2,1)S(1)} %copy-done, f32[512,256]{0,1:T(8,128)} %fusion.2, f32[512]{0:T(512)S(1)} %add_rsqrt_fusion), kind=kOutput, calls=%fused_computation.1 | convolution fusion | flops 1075707904 | bytes 6817792 | tf_op jit(solution)/shard_map/dot_general | solution.py:73
  159.7 3.2 %copy.16 = bf16[2,16,16,2048]{3,2,1,0:T(8,128)(2,1)} copy(bf16[2,16,16,2048]{3,2,0,1:T(8,128)(2,1)} %bitcast.28) | data formatting | bytes 4194304 | tf_op jit(solution)/shard_map/transpose | solution.py:40
  162.8 0.0 reduce-scatter.5.cloned.1.call-start
  162.9 16.7 %reduce-scatter.3.cloned.1.call-done = bf16[16,16,2048]{2,1,0:T(8,128)(2,1)} async-done(((bf16[32,16,2048]{2,1,0:T(8,128)(2,1)}), bf16[16,16,2048]{2,1,0:T(8,128)(2,1)}) %reduce-scatter.3.cloned.1.call-update) | async-done | bytes 1048592 | tf_op jit(solution)/shard_map/reduce_scatter | solution.py:43
  179.6 1.4 copy.17
  181.0 74.5 %reduce-scatter.5.cloned.1.call-done = bf16[1,16,2048]{2,1,0:T(8,128)(2,1)} async-done(((bf16[16,16,2048]{2,1,0:T(8,128)(2,1)}), bf16[1,16,2048]{2,1,0:T(8,128)(2,1)}) %reduce-scatter.5.cloned.1.call-update) | async-done | bytes 65552 | tf_op jit(solution)/shard_map/reduce_scatter | solution.py:43
  (8 shorter events, 0.1 us)
Async XLA Ops:
  7.2 68.8 %all-gather.3.cloned.1.call-start = ((), (), s32[]{:S(2)}) async-start(), calls=%async_computation.4 | async-start | bytes 2228224 | tf_op jit(solution)/shard_map/all_gather | solution.py:15
  11.0 23.7 %all-to-all-start = ((bf16[16,512,64]{1,2,0:T(8,128)(2,1)}), bf16[16,512,64]{1,2,0:T(8,128)(2,1)S(1)}, u32[]{:S(2)}, u32[]{:S(2)}) async-start(bf16[16,512,64]{1,2,0:T(8,128)(2,1)} %broadcast_in_dim.2), calls=%async_computation | async-start | bytes 2097152 | tf_op jit(solution)/shard_map/all_to_all | solution.py:30
  20.3 130.1 %all-gather.5.cloned.1.call-start = ((), (), s32[]{:S(2)}) async-start(), calls=%async_computation.5 | async-start | bytes 2162688 | tf_op jit(solution)/shard_map/all_gather | solution.py:61
  37.2 118.3 %all-to-all-start.1 = ((bf16[32,256,64]{1,2,0:T(8,128)(2,1)}), bf16[32,256,64]{1,2,0:T(8,128)(2,1)S(1)}, u32[]{:S(2)}, u32[]{:S(2)}) async-start(bf16[32,256,64]{1,2,0:T(8,128)(2,1)} %copy.15), calls=%async_computation.1 | async-start | bytes 2097152 | tf_op jit(solution)/shard_map/all_to_all | solution.py:68
  52.3 127.3 %reduce-scatter.3.cloned.1.call-start = ((), (), s32[]{:S(2)}) async-start(), calls=%async_computation.6 | async-start | bytes 3145728 | tf_op jit(solution)/shard_map/reduce_scatter | solution.py:43
  150.4 2.3 copy-start
  162.8 92.6 %reduce-scatter.5.cloned.1.call-start = ((), (), s32[]{:S(2)}) async-start(), calls=%async_computation.7 | async-start | bytes 1114112 | tf_op jit(solution)/shard_map/reduce_scatter | solution.py:43
Sparse Core Ops, SparseCore 0:
  11.6 64.3 all-gather.2
  78.1 72.3 all-gather.4
  163.0 16.5 reduce-scatter.2
  182.8 72.6 reduce-scatter.4
where the time goes:
time: 262 us
  waiting for transfers between devices  201 us (77%)
  starting transfers between devices  24.5 us (9%)
  between operations  13.8 us (5%)
  local copies, waits for them, and re-layouts  11.2 us (4%)
  matrix products  6.97 us (3%)
  other arithmetic  4.91 us (2%)
    reduce_scatter x2, waiting for transfers between devices, sum_in_order(): pieces = lax.psum_scatter(pieces, axes[k], scatter_dimension=0, tiled=True)  91.2 us
    all_gather x1, waiting for transfers between devices, body(): features = lax.all_gather(tokens, TP, axis=1, tiled=True)  71.5 us
    all_gather x1, waiting for transfers between devices, side_by_side(): lax.all_gather(both, axis, axis=dim, tiled=True)  23.6 us
    all_to_all x1, starting transfers between devices, body(): lax.all_to_all(down_rows, TP, split_axis=0, concat_axis=1, tiled=True)  15 us
    all_to_all x1, waiting for transfers between devices, copy_for_each(): return lax.all_to_all(copies, axis, split_axis=0, concat_axis=0, tiled=True)  13.6 us
    all_to_all x1, starting transfers between devices, copy_for_each(): return lax.all_to_all(copies, axis, split_axis=0, concat_axis=0, tiled=True)  9.32 us
  transfers between devices with their start and end apart: 6, of which 5 were waited for; matrix products, arithmetic and copies ran while one was open for 5% of the time, Pallas kernels for 0%

commit v1 on v0

--- a/solution.py
+++ b/solution.py
@@ -65,7 +65,9 @@
     gate_sum = jnp.dot(features, gate_whole, preferred_element_type=jnp.float32)
     up_sum = jnp.dot(features, up_whole, preferred_element_type=jnp.float32)
     down_rows = collect(down_local, "fs", 0)
-    down_whole = lax.all_to_all(down_rows, TP, split_axis=0, concat_axis=1, tiled=True)
+    down_whole = jnp.concatenate(
+        lax.all_to_all(jnp.stack(jnp.split(down_rows, lax.axis_size(TP), axis=0)), TP, 0, 0), axis=1
+    )
     scale = lax.rsqrt(squares / D + epsilon)[:, None]
     hidden = (jax.nn.silu(gate_sum * scale) * (up_sum * scale)).astype(jnp.bfloat16)
     mixed = (

time: 262 us -> 269 us (1.027)
  local copies, waits for them, and re-layouts: 11.2 us -> 28.6 us
  waiting for transfers between devices: 201 us -> 190 us
    unnamed x3 -> x34, local copies, waits for them, and re-layouts: 1.43 us -> 20.6 us
    all_gather x1, waiting for transfers between devices: 23.6 us -> 6.24 us  [side_by_side(): lax.all_gather(both, axis, axis=dim, tiled=True)]
    all_gather x1, waiting for transfers between devices: 71.5 us -> 77.7 us  [body(): features = lax.all_gather(tokens, TP, axis=1, tiled=True)]
  transfers between devices with their start and end apart: 6 -> 6, of which waited for: 5 -> 5; matrix products, arithmetic and copies ran while one was open for 5% -> 12% of each run, Pallas kernels for 0% -> 0%
where the time goes in v1:
time: 269 us; the launch traced here: 268 us
  waiting for transfers between devices  190 us (71%)
  local copies, waits for them, and re-layouts  28.6 us (11%)
  starting transfers between devices  24.5 us (9%)
  between operations  13.8 us (5%)
  matrix products  6.96 us (3%)
  other arithmetic  4.91 us (2%)
    reduce_scatter x2, waiting for transfers between devices, sum_in_order(): pieces = lax.psum_scatter(pieces, axes[k], scatter_dimension=0, tiled=True)  91.5 us
    all_gather x1, waiting for transfers between devices, body(): features = lax.all_gather(tokens, TP, axis=1, tiled=True)  77.7 us
    unnamed x34, local copies, waits for them, and re-layouts  20.6 us
    all_to_all x1, starting transfers between devices, body(): lax.all_to_all(jnp.stack(jnp.split(down_rows, lax.axis_size(TP), axis=0))...  15 us
    all_to_all x1, waiting for transfers between devices, copy_for_each(): return lax.all_to_all(copies, axis, split_axis=0, concat_axis=0, tiled=True)  13.6 us
    all_to_all x1, starting transfers between devices, copy_for_each(): return lax.all_to_all(copies, axis, split_axis=0, concat_axis=0, tiled=True)  9.32 us
    all_gather x1, waiting for transfers between devices, side_by_side(): lax.all_gather(both, axis, axis=dim, tiled=True)  6.24 us
  transfers between devices with their start and end apart: 6, of which 5 were waited for; matrix products, arithmetic and copies ran while one was open for 12% of the time, Pallas kernels for 0%

profile of v1, /device:TPU:2, one launch (start us, length us, event | category | flops | bytes accessed | tf_op | source)
XLA Modules:
  0.0 268.5 jit_solution(5697342496282210753)
XLA Ops:
  7.2 1.1 multiply_convert_fusion.1
  8.3 0.7 pad_maximum_fusion
  9.0 0.9 convert_element_type.22
  9.9 1.1 broadcast_in_dim.2
  11.0 9.3 %all-to-all-start = ((bf16[16,512,64]{1,2,0:T(8,128)(2,1)}), bf16[16,512,64]{1,2,0:T(8,128)(2,1)S(1)}, u32[]{:S(2)}, u32[]{:S(2)}) async-start(bf16[16,512,64]{1,2,0:T(8,128)(2,1)} %broadcast_in_dim.2), calls=%async_computation | async-start | bytes 2097152 | tf_op jit(solution)/shard_map/all_to_all | solution.py:30
  20.3 0.7 all-gather.5.cloned.1.call-update
  21.0 13.6 %all-to-all-done = bf16[16,512,64]{1,2,0:T(8,128)(2,1)S(1)} async-done(((bf16[16,512,64]{1,2,0:T(8,128)(2,1)}), bf16[16,512,64]{1,2,0:T(8,128)(2,1)S(1)}, u32[]{:S(2)}, u32[]{:S(2)}) %all-to-all-start) | async-done | bytes 1048608 | tf_op jit(solution)/shard_map/all_to_all | solution.py:30
  34.8 0.6 constant_dynamic-update-slice_fusion.31
  35.4 0.6 constant_dynamic-update-slice_fusion.30
  37.2 0.6 constant_dynamic-update-slice_fusion.27
  39.1 0.6 constant_dynamic-update-slice_fusion.24
  41.0 0.6 constant_dynamic-update-slice_fusion.21
  42.8 0.6 constant_dynamic-update-slice_fusion.18
  54.6 15.0 %all-to-all-start.1 = ((bf16[32,256,64]{1,2,0:T(8,128)(2,1)}), bf16[32,256,64]{1,2,0:T(8,128)(2,1)S(1)}, u32[]{:S(2)}, u32[]{:S(2)}) async-start(bf16[32,256,64]{1,2,0:T(8,128)(2,1)} %constant_dynamic-update-slice_fusion), calls=%async_computation.1 | async-start | bytes 2097152 | tf_op jit(solution)/shard_map/all_to_all | solution.py:69
  69.7 6.2 %all-gather.3.cloned.1.call-done = bf16[2048,512]{1,0:T(8,128)(2,1)} async-done(((bf16[128,512]{1,0:T(8,128)(2,1)}), bf16[2048,512]{1,0:T(8,128)(2,1)}) %all-gather.3.cloned.1.call-update) | async-done | bytes 2097168 | tf_op jit(solution)/shard_map/all_gather | solution.py:15
  75.9 3.0 %fusion.12 = (bf16[2048,256]{1,0:T(8,128)(2,1)}, bf16[2048,256]{1,0:T(8,128)(2,1)}) fusion(bf16[2048,512]{1,0:T(8,128)(2,1)} %all-gather.3.cloned.1.call-done), kind=kLoop, calls=%fused_computation.84 | loop fusion | bytes 4194304 | tf_op jit(solution)/shard_map/slice | solution.py:17
  78.9 77.7 %all-gather.5.cloned.1.call-done = bf16[512,2048]{0,1:T(8,128)(2,1)} async-done(((bf16[512,64]{0,1:T(8,128)(2,1)}), bf16[512,2048]{0,1:T(8,128)(2,1)}) %all-gather.5.cloned.1.call-update) | async-done | bytes 2097168 | tf_op jit(solution)/shard_map/all_gather | solution.py:61
  156.6 2.2 multiply_reduce_fusion
  158.9 2.8 %fusion.2 = f32[512,256]{0,1:T(8,128)} fusion(bf16[2048,256]{1,0:T(8,128)(2,1)} %get-tuple-element.13, bf16[512,2048]{0,1:T(8,128)(2,1)S(1)} %copy-done, f32[512]{0:T(512)S(1)} %add_rsqrt_fusion), kind=kOutput, calls=%fused_computation.6 | convolution fusion | flops 537001984 | bytes 3672064 | tf_op jit(solution)/shard_map/dot_general | solution.py:65
  161.6 4.2 %convolution_convert_fusion = bf16[512,2048]{1,0:T(8,128)(2,1)} fusion(bf16[256,2048]{0,1:T(8,128)(2,1)S(1)} %bitcast.186, bf16[2048,256]{1,0:T(8,128)(2,1)} %get-tuple-element.12, bf16[512,2048]{0,1:T(8,128)(2,1)S(1)} %copy-done, f32[512,256]{0,1:T(8,128)} %fusion.2, f32[512]{0:T(512)S(1)} %add_rsqrt_fusion), kind=kOutput, calls=%fused_computation.1 | convolution fusion | flops 1075707904 | bytes 6817792 | tf_op jit(solution)/shard_map/dot_general | solution.py:75
  165.8 3.2 %copy.45 = bf16[2,16,16,2048]{3,2,1,0:T(8,128)(2,1)} copy(bf16[2,16,16,2048]{3,2,0,1:T(8,128)(2,1)} %bitcast.189) | data formatting | bytes 4194304 | tf_op jit(solution)/shard_map/transpose | solution.py:40
  169.1 16.9 %reduce-scatter.3.cloned.1.call-done = bf16[16,16,2048]{2,1,0:T(8,128)(2,1)} async-done(((bf16[32,16,2048]{2,1,0:T(8,128)(2,1)}), bf16[16,16,2048]{2,1,0:T(8,128)(2,1)}) %reduce-scatter.3.cloned.1.call-update) | async-done | bytes 1048592 | tf_op jit(solution)/shard_map/reduce_scatter | solution.py:43
  186.0 1.4 copy.46
  187.4 74.5 %reduce-scatter.5.cloned.1.call-done = bf16[1,16,2048]{2,1,0:T(8,128)(2,1)} async-done(((bf16[16,16,2048]{2,1,0:T(8,128)(2,1)}), bf16[1,16,2048]{2,1,0:T(8,128)(2,1)}) %reduce-scatter.5.cloned.1.call-update) | async-done | bytes 65552 | tf_op jit(solution)/shard_map/reduce_scatter | solution.py:43
  (38 shorter events, 16.4 us)
Async XLA Ops:
  7.2 68.8 %all-gather.3.cloned.1.call-start = ((), (), s32[]{:S(2)}) async-start(), calls=%async_computation.4 | async-start | bytes 2228224 | tf_op jit(solution)/shard_map/all_gather | solution.py:15
  11.0 23.7 %all-to-all-start = ((bf16[16,512,64]{1,2,0:T(8,128)(2,1)}), bf16[16,512,64]{1,2,0:T(8,128)(2,1)S(1)}, u32[]{:S(2)}, u32[]{:S(2)}) async-start(bf16[16,512,64]{1,2,0:T(8,128)(2,1)} %broadcast_in_dim.2), calls=%async_computation | async-start | bytes 2097152 | tf_op jit(solution)/shard_map/all_to_all | solution.py:30
  20.3 136.3 %all-gather.5.cloned.1.call-start = ((), (), s32[]{:S(2)}) async-start(), calls=%async_computation.5 | async-start | bytes 2162688 | tf_op jit(solution)/shard_map/all_gather | solution.py:61
  54.6 107.0 %all-to-all-start.1 = ((bf16[32,256,64]{1,2,0:T(8,128)(2,1)}), bf16[32,256,64]{1,2,0:T(8,128)(2,1)S(1)}, u32[]{:S(2)}, u32[]{:S(2)}) async-start(bf16[32,256,64]{1,2,0:T(8,128)(2,1)} %constant_dynamic-update-slice_fusion), calls=%async_computation.1 | async-start | bytes 2097152 | tf_op jit(solution)/shard_map/all_to_all | solution.py:69
  69.6 116.3 %reduce-scatter.3.cloned.1.call-start = ((), (), s32[]{:S(2)}) async-start(), calls=%async_computation.6 | async-start | bytes 3145728 | tf_op jit(solution)/shard_map/reduce_scatter | solution.py:43
  156.6 2.3 copy-start
  169.0 93.0 %reduce-scatter.5.cloned.1.call-start = ((), (), s32[]{:S(2)}) async-start(), calls=%async_computation.7 | async-start | bytes 1114112 | tf_op jit(solution)/shard_map/reduce_scatter | solution.py:43
Sparse Core Ops, SparseCore 0:
  11.6 64.3 all-gather.2
  78.1 78.4 all-gather.4
  169.1 16.8 reduce-scatter.2
  189.2 72.7 reduce-scatter.4
